TPU v7x, 256 devices: a 8x8x2 block of a 8x8x16 slice. The times are simulated.
256 devices in a mesh: grp: 2 (over z), ep: 16 (over y, core), tp: 8 (over x).
Axes of the slice: x: 8, y: 8, z: 2, core: 2. Of those that a mesh axis runs over, the one named last changes fastest.
The devices are a block of a 8x8x16 slice.
Arguments:
- pool_input: bfloat16 [32768, 1024], P(('grp', 'ep'), 'tp'), parts along dimension 0, may hold values from -6 to 6
- pool_map: bfloat16 [8, 128, 128], replicated, may hold values from -0.5 to 0.5
- pool_scale: float32 [1024], replicated, may hold values from 0.1 to 1.9
- out_weight: bfloat16 [1024, 2048], P(None, 'tp'), may hold values from -0.1875 to 0.1875
- expert_input: bfloat16 [32768, 2048], P(('grp', 'ep', 'tp')), parts along dimension 0, may hold values from -6 to 6
- norm_gain: float32 [2048], replicated, may hold values from 0.1 to 1.9
- routes: int32 [32768, 2], P(('grp', 'ep', 'tp')), parts along dimension 0, may hold values from 0 to 127, all different within a row; in each aligned block of 128 rows (0 to 127, 128 to 255, ...) at most 4 rows name the same one
- route_weight: float32 [32768, 2], P(('grp', 'ep', 'tp')), parts along dimension 0, may hold values from 0.2 to 1.5
- gate_weight: bfloat16 [128, 2048, 512], P(('ep', 'tp')), may hold values from -0.125 to 0.125
- up_weight: bfloat16 [128, 2048, 512], P(('ep', 'tp')), may hold values from -0.125 to 0.125
- down_weight: bfloat16 [128, 512, 2048], P(('ep', 'tp')), may hold values from -0.25 to 0.25
Outputs:
- pool_output: bfloat16 [32768, 2048], P(('grp', 'ep'), 'tp'), parts along dimension 0
- expert_output: bfloat16 [32768, 2048], P(('grp', 'ep', 'tp')), parts along dimension 0
There are 2 independent parts, one for each index of `grp`. A program takes and returns all parts, laid end to end along the dimension named above; an argument that names none is the same for every part. Nothing has to cross between parts.
Inputs may be any that keep to these rules, and one draw needn't show every extreme that they name: `routes`: each row names 2 different experts. In the rows of one device no expert is named more than 4 times, and in every draw some device names some expert exactly 4 times.
All inputs are finite; a program needn't handle non-finite values.
Results may differ from a plain program's by a relative error of at most 0.007.
Values may be sent and summed in bfloat16 or wider, within the bound.
A program may use at most 64 MiB of HBM per device.

v0:
```python
import jax
import jax.numpy as jnp
from jax import lax
from jax.sharding import PartitionSpec as P

epsilon = 1e-06
halo_depth = 16


def shifted_2(shard, axis, by):
    size = lax.axis_size(axis)
    pairs = [(i, i + by) for i in range(size) if 0 <= i + by < size]
    return lax.ppermute(shard, axis, pairs)


def expert_rows(received, gate_weight, up_weight, down_weight):
    shape_in = received.shape
    flat_rows = received.reshape(-1, shape_in[-1])
    gate_part = jnp.dot(flat_rows, gate_weight[0], preferred_element_type=jnp.float32)
    up_part = jnp.dot(flat_rows, up_weight[0], preferred_element_type=jnp.float32)
    hidden = (jax.nn.silu(gate_part) * up_part).astype(jnp.bfloat16)
    result = jnp.dot(hidden, down_weight[0], preferred_element_type=jnp.float32).astype(
        jnp.bfloat16
    )
    return result.reshape(shape_in)


def pool_half(pool_input, pool_map, pool_scale, out_weight):
    row_count, width_local = pool_input.shape
    group_dim = pool_map.shape[1]
    groups_local = width_local // group_dim
    last_rows = pool_input[row_count - halo_depth :]
    earlier_rows = shifted_2(last_rows, "ep", 1)
    extended = jnp.concatenate([earlier_rows, pool_input], axis=0).astype(jnp.float32)
    first_group = lax.axis_index("tp") * groups_local
    group_ids = first_group + jnp.arange(width_local, dtype=jnp.int32) // group_dim
    window = jnp.left_shift(jnp.int32(2), group_ids % 4)
    summed = jnp.zeros((row_count, width_local), jnp.float32)
    for offset in range(halo_depth):
        shifted = extended[halo_depth - offset : halo_depth - offset + row_count]
        summed = summed + jnp.where(offset < window, shifted, 0.0)
    positions = lax.axis_index("ep") * row_count + jnp.arange(row_count, dtype=jnp.int32)
    counted = jnp.minimum(positions[:, None] + 1, window[None, :]).astype(jnp.float32)
    pooled = (summed / counted - extended[halo_depth:]).astype(jnp.bfloat16)
    maps_local = lax.dynamic_slice_in_dim(pool_map, first_group, groups_local, 0)
    scales_local = lax.dynamic_slice_in_dim(pool_scale, first_group * group_dim, width_local, 0)
    mapped = jnp.einsum(
        "rgc,gcd->rgd",
        pooled.reshape(row_count, groups_local, group_dim),
        maps_local,
        preferred_element_type=jnp.float32,
    )
    mapped = (mapped.reshape(row_count, width_local) * scales_local).astype(jnp.bfloat16)
    projected = jnp.dot(
        lax.all_gather(mapped, "tp", axis=1, tiled=True),
        out_weight,
        preferred_element_type=jnp.float32,
    )
    return projected.astype(jnp.bfloat16)


def expert_half(expert_input, norm_gain, routes, route_weight, gate_weight, up_weight, down_weight):
    row_count, model_width = expert_input.shape
    top_count = routes.shape[1]
    widened = expert_input.astype(jnp.float32)
    normed = (
        widened
        * lax.rsqrt(jnp.mean(widened * widened, axis=1, keepdims=True) + epsilon)
        * norm_gain
    )
    normed = normed.astype(jnp.bfloat16)
    ep_count = lax.axis_size("ep")
    tp_count = lax.axis_size("tp")
    experts = ep_count * tp_count
    capacity = 2 * row_count * top_count // experts
    copies = row_count * top_count
    flat_routes = routes.reshape(copies)
    onehot = (flat_routes[:, None] == jnp.arange(experts, dtype=jnp.int32)[None, :]).astype(
        jnp.int32
    )
    slot_index = jnp.sum((jnp.cumsum(onehot, axis=0) - onehot) * onehot, axis=1)
    target = flat_routes * capacity + slot_index
    source_row = jnp.arange(copies, dtype=jnp.int32) // top_count
    slot_table = jnp.full((experts * capacity,), row_count, jnp.int32).at[target].set(source_row)
    padded = jnp.concatenate([normed, jnp.zeros((1, model_width), jnp.bfloat16)], axis=0)
    outgoing = padded[slot_table].reshape(experts, capacity, model_width)
    results = expert_rows(
        lax.all_to_all(outgoing, ("ep", "tp"), split_axis=0, concat_axis=0, tiled=True),
        gate_weight,
        up_weight,
        down_weight,
    )
    returned = lax.all_to_all(results, ("ep", "tp"), split_axis=0, concat_axis=0, tiled=True)
    returned = returned.reshape(experts * capacity, model_width)
    picked = returned[target].astype(jnp.float32) * route_weight.reshape(copies)[:, None]
    return picked.reshape(row_count, top_count, model_width).sum(axis=1).astype(jnp.bfloat16)


def on_device(
    pool_input,
    pool_map,
    pool_scale,
    out_weight,
    expert_input,
    norm_gain,
    routes,
    route_weight,
    gate_weight,
    up_weight,
    down_weight,
):
    pool_output = pool_half(pool_input, pool_map, pool_scale, out_weight)
    expert_output = expert_half(
        expert_input, norm_gain, routes, route_weight, gate_weight, up_weight, down_weight
    )
    return (pool_output, expert_output)


def solution(mesh):
    return jax.shard_map(
        on_device,
        mesh=mesh,
        in_specs=(
            P(("grp", "ep"), "tp"),
            P(),
            P(),
            P(None, "tp"),
            P(("grp", "ep", "tp"), None),
            P(),
            P(("grp", "ep", "tp"), None),
            P(("grp", "ep", "tp"), None),
            P(("ep", "tp"), None, None),
            P(("ep", "tp"), None, None),
            P(("ep", "tp"), None, None),
        ),
        out_specs=(P(("grp", "ep"), "tp"), P(("grp", "ep", "tp"), None)),
        check_vma=False,
    )
```

profile of v0, /device:TPU:528, one launch (start us, length us, event | category | flops | bytes accessed | tf_op | source)
XLA Modules:
  0.0 223.0 jit_solution(10433122955356067923)
XLA Ops:
  7.2 0.0 copy-start
  7.2 0.0 copy-start.1
  7.2 0.9 copy.15
  8.1 0.1 eq.31
  8.3 0.1 eq.27
  8.4 0.7 broadcast_multiply_fusion
  9.1 0.1 copy.17
  9.2 0.2 fusion.38
  9.5 0.1 copy.14
  9.6 0.1 mul.79
  9.8 0.2 fusion.40
  10.0 1.4 scatter_custom_fusion
  11.4 1.2 fusion.13
  12.7 0.0 copy-done.1
  12.7 0.9 fusion.15
  13.6 3.3 %gather_fusion = bf16[512,2048]{1,0:T(8,128)(2,1)} fusion(bf16[129,2048]{1,0:T(8,128)(2,1)S(1)} %concatenate.7, s32[1024]{0:T(1024)S(1)} %pad_clamp_fusion.1), kind=kCustom, calls=%fused_computation | custom fusion | bytes 4196352 | tf_op jit(solution)/shard_map/gather | solution.py:86
  16.9 4.1 %reshape.127 = bf16[128,4,2048]{2,1,0:T(4,128)(2,1)} reshape(bf16[512,2048]{1,0:T(8,128)(2,1)} %gather_fusion) | data formatting | bytes 4194304 | tf_op jit(solution)/shard_map/reshape | solution.py:86
  21.0 0.0 copy-start.2
  21.0 26.4 %all-to-all-start = ((bf16[128,4,2048]{2,1,0:T(4,128)(2,1)}), bf16[128,4,2048]{2,1,0:T(4,128)(2,1)}, u32[]{:S(2)}, u32[]{:S(2)}) async-start(bf16[128,4,2048]{2,1,0:T(4,128)(2,1)} %reshape.127), calls=%async_computation | async-start | bytes 4194304 | tf_op jit(solution)/shard_map/all_to_all | solution.py:88
  47.4 0.0 copy-done.2
  47.4 2.2 collective-permute-start
  49.8 0.8 dynamic_slice.7
  50.6 5.9 %collective-permute-done = bf16[16,128]{1,0:T(8,128)(2,1)S(1)} collective-permute-done((bf16[16,128]{1,0:T(8,128)(2,1)S(1)}, bf16[16,128]{1,0:T(8,128)(2,1)S(1)}, u32[]{:S(2)}, u32[]{:S(2)}) %collective-permute-start) | collective-permute-done | bytes 4128 | tf_op jit(solution)/shard_map/ppermute | solution.py:13
  56.5 42.0 %all-to-all-done = bf16[128,4,2048]{2,1,0:T(4,128)(2,1)} async-done(((bf16[128,4,2048]{2,1,0:T(4,128)(2,1)}), bf16[128,4,2048]{2,1,0:T(4,128)(2,1)}, u32[]{:S(2)}, u32[]{:S(2)}) %all-to-all-start) | async-done | bytes 2097184 | tf_op jit(solution)/shard_map/all_to_all | solution.py:88
  98.5 3.9 %reshape.128 = bf16[512,2048]{1,0:T(8,128)(2,1)} reshape(bf16[128,4,2048]{2,1,0:T(4,128)(2,1)} %all-to-all-done) | data formatting | bytes 4194304 | tf_op jit(solution)/shard_map/reshape | solution.py:18
  102.4 4.5 %fusion.3 = f32[512,512]{1,0:T(8,128)} fusion(bf16[512,2048]{1,0:T(8,128)(2,1)} %reshape.128, bf16[1,2048,512]{2,1,0:T(8,128)(2,1)} %param.19), kind=kOutput, calls=%fused_computation.7 | convolution fusion | flops 1073741824 | bytes 5242880 | tf_op jit(solution)/shard_map/dot_general | solution.py:19
  106.9 0.0 copy-done
  106.9 6.2 %convolution_convert_fusion = bf16[512,2048]{1,0:T(8,128)(2,1)} fusion(bf16[1,512,2048]{2,1,0:T(8,128)(2,1)S(1)} %copy-done, bf16[512,2048]{1,0:T(8,128)(2,1)} %reshape.128, bf16[1,2048,512]{2,1,0:T(8,128)(2,1)} %param.20, f32[512,512]{1,0:T(8,128)} %fusion.3), kind=kOutput, calls=%fused_computation.3 | convolution fusion | flops 2150105088 | bytes 9437184 | tf_op jit(solution)/shard_map/dot_general | solution.py:22
  113.1 4.1 %reshape.129 = bf16[128,4,2048]{2,1,0:T(4,128)(2,1)} reshape(bf16[512,2048]{1,0:T(8,128)(2,1)} %convolution_convert_fusion) | data formatting | bytes 4194304 | tf_op jit(solution)/shard_map/reshape | solution.py:25
  117.2 9.9 %all-to-all-start.1 = ((bf16[128,4,2048]{2,1,0:T(4,128)(2,1)}), bf16[128,4,2048]{2,1,0:T(4,128)(2,1)}, u32[]{:S(2)}, u32[]{:S(2)}) async-start(bf16[128,4,2048]{2,1,0:T(4,128)(2,1)} %reshape.129), calls=%async_computation.1 | async-start | bytes 4194304 | tf_op jit(solution)/shard_map/all_to_all | solution.py:93
  127.1 0.1 all-gather.2.cloned.1.call-start
  127.2 0.0 copy-start.3
  127.2 3.5 %fusion.12 = bf16[1024,128]{0,1:T(8,128)(2,1)} fusion(f32[128]{0:T(128)S(1)} %dynamic_slice.7, f32[1040,128]{1,0:T(8,128)S(1)} %maximum_convert_fusion, s32[128]{0:T(128)S(1)} %fusion.48, s32[1024]{0:T(1024)S(1)} %add_add_fusion, pred[128]{0:T(512)(128)(4,1)S(1)} %get-tuple-element.2, pred[128]{0:T(512)(128)(4,1)S(1)} %get-tuple-element.3, ...), kind=kOutput, calls=%fused_computation.17 | convolution fusion | flops 38535168 | bytes 8696836 | tf_op jit(solution)/shard_map/rgc,gcd->rgd/dot_general | solution.py:47
  130.7 0.1 all-gather.2.cloned.1.call-update
  130.8 0.0 copy-done.3
  130.8 0.1 copy.19
  130.9 65.9 %all-gather.2.cloned.1.call-done = bf16[1024,1024]{0,1:T(8,128)(2,1)} async-done(((bf16[1024,128]{0,1:T(8,128)(2,1)}), bf16[1024,1024]{0,1:T(8,128)(2,1)}) %all-gather.2.cloned.1.call-update) | async-done | bytes 2097168 | tf_op jit(solution)/shard_map/all_gather | solution.py:55
  196.8 3.2 %convolution_convert_fusion.1 = bf16[1024,256]{1,0:T(8,128)(2,1)} fusion(bf16[1024,1024]{0,1:T(8,128)(2,1)} %all-gather.2.cloned.1.call-done, bf16[1024,256]{1,0:T(8,128)(2,1)} %param.14), kind=kOutput, calls=%fused_computation.13 | convolution fusion | flops 537133056 | bytes 3145728 | tf_op jit(solution)/shard_map/dot_general | solution.py:54
  200.0 0.0 all-to-all-done.1
  200.0 3.9 %reshape.130 = bf16[512,2048]{1,0:T(8,128)(2,1)} reshape(bf16[128,4,2048]{2,1,0:T(4,128)(2,1)} %all-to-all-done.1) | data formatting | bytes 4194304 | tf_op jit(solution)/shard_map/reshape | solution.py:94
  203.9 4.2 %gather_fusion.1 = bf16[256,2048]{1,0:T(8,128)(2,1)S(1)} fusion(bf16[512,2048]{1,0:T(8,128)(2,1)} %reshape.130, s32[1024]{0:T(1024)S(1)} %pad_clamp_fusion), kind=kCustom, calls=%fused_computation.1 | custom fusion | bytes 2098176 | tf_op jit(solution)/shard_map/gather | solution.py:95
  208.2 2.3 %reshape.131 = f32[128,2,2048]{2,1,0:T(2,128)} reshape(bf16[256,2048]{1,0:T(8,128)(2,1)S(1)} %gather_fusion.1) | data formatting | bytes 3145728 | tf_op jit(solution)/shard_map/convert_element_type | solution.py:95
  210.5 5.6 %multiply_reduce_fusion = bf16[128,2048]{1,0:T(8,128)(2,1)} fusion(f32[128,2,2048]{2,1,0:T(2,128)} %reshape.131, f32[128,2]{1,0:T(8,128)S(1)} %copy.19), kind=kLoop, calls=%fused_computation.9 | loop fusion | flops 786432 | bytes 2622464 | tf_op jit(solution)/shard_map/reduce_sum | solution.py:96
  (25 shorter events, 0.3 us)
Async XLA Ops:
  7.2 99.7 %copy-start = (bf16[1,512,2048]{2,1,0:T(8,128)(2,1)S(1)}, bf16[1,512,2048]{2,1,0:T(8,128)(2,1)}, u32[]{:S(2)}) copy-start(bf16[1,512,2048]{2,1,0:T(8,128)(2,1)} %param.21) | copy-start | bytes 6291460
  7.2 5.5 %copy-start.1 = (bf16[128,2048]{1,0:T(8,128)(2,1)S(1)}, bf16[128,2048]{1,0:T(8,128)(2,1)}, u32[]{:S(2)}) copy-start(bf16[128,2048]{1,0:T(8,128)(2,1)} %param.15) | copy-start | bytes 1572868
  21.0 26.4 %copy-start.2 = (bf16[1024,128]{1,0:T(8,128)(2,1)S(1)}, bf16[1024,128]{1,0:T(8,128)(2,1)}, u32[]{:S(2)}) copy-start(bf16[1024,128]{1,0:T(8,128)(2,1)} %param.11) | copy-start | bytes 786436
  21.0 77.5 %all-to-all-start = ((bf16[128,4,2048]{2,1,0:T(4,128)(2,1)}), bf16[128,4,2048]{2,1,0:T(4,128)(2,1)}, u32[]{:S(2)}, u32[]{:S(2)}) async-start(bf16[128,4,2048]{2,1,0:T(4,128)(2,1)} %reshape.127), calls=%async_computation | async-start | bytes 4194304 | tf_op jit(solution)/shard_map/all_to_all | solution.py:88
  47.4 9.0 %collective-permute-start = (bf16[16,128]{1,0:T(8,128)(2,1)S(1)}, bf16[16,128]{1,0:T(8,128)(2,1)S(1)}, u32[]{:S(2)}, u32[]{:S(2)}) collective-permute-start(bf16[16,128]{1,0:T(8,128)(2,1)S(1)} %slice.58), channel_id=1, source_target_pairs={{0,8},{8,16},{16,24},{24,32},{32,40},{40,48},{48,56},{56,64},{64,7... | collective-permute-start | bytes 12296 | tf_op jit(solution)/shard_map/ppermute | solution.py:13
  117.2 82.8 %all-to-all-start.1 = ((bf16[128,4,2048]{2,1,0:T(4,128)(2,1)}), bf16[128,4,2048]{2,1,0:T(4,128)(2,1)}, u32[]{:S(2)}, u32[]{:S(2)}) async-start(bf16[128,4,2048]{2,1,0:T(4,128)(2,1)} %reshape.129), calls=%async_computation.1 | async-start | bytes 4194304 | tf_op jit(solution)/shard_map/all_to_all | solution.py:93
  127.1 69.7 %all-gather.2.cloned.1.call-start = ((), (), s32[]{:S(2)}) async-start(), calls=%async_computation.2 | async-start | bytes 2359296 | tf_op jit(solution)/shard_map/all_gather | solution.py:55
  127.2 3.6 %copy-start.3 = (f32[128,2]{0,1:T(2,128)S(1)}, f32[128,2]{0,1:T(2,128)}, u32[]{:S(2)}) copy-start(f32[128,2]{0,1:T(2,128)} %param.18) | copy-start | bytes 3076
Sparse Core Ops, SparseCore 0:
  130.9 65.8 all-gather.1
where the time goes:
time: 224 us; the launch traced here: 223 us
  waiting for transfers between devices  114 us (51%)
  starting transfers between devices  38.5 us (17%)
  local copies, waits for them, and re-layouts  29.9 us (13%)
  matrix products  17.4 us (8%)
  between operations  14.3 us (6%)
  other arithmetic  9.04 us (4%)
    all_gather x1, waiting for transfers between devices, pool_half(): lax.all_gather(mapped, 'tp', axis=1, tiled=True)  65.9 us
    all_to_all x1, waiting for transfers between devices, expert_half(): lax.all_to_all(outgoing, ('ep', 'tp'), split_axis=0, concat_axis=0, tiled...  42 us
    all_to_all x1, starting transfers between devices, expert_half(): lax.all_to_all(outgoing, ('ep', 'tp'), split_axis=0, concat_axis=0, tiled...  26.4 us
    all_to_all x1, starting transfers between devices, expert_half(): lax.all_to_all(results, ('ep', 'tp'), split_axis=0, concat_axis=0, tiled=...  9.88 us
    dot_general x1, matrix products, expert_rows(): jnp.dot(hidden, down_weight[0], preferred_element_type=jnp.float32)  6.23 us
    ppermute x1, waiting for transfers between devices, shifted_2(): return lax.ppermute(shard, axis, pairs)  5.87 us
    reduce_sum x1, other arithmetic, expert_half(): picked.reshape(row_count, top_count, model_width).sum(axis=1)  5.59 us
  transfers between devices with their start and end apart: 4, of which 3 were waited for; matrix products, arithmetic and copies ran while one was open for 4% of the time, Pallas kernels for 0%

commit v1 on v0

v1 whole, which is shorter than its diff:
```python
import functools

import jax
import jax.numpy as jnp
from jax import lax
from jax.experimental import pallas as pl
from jax.experimental.pallas import tpu as pltpu
from jax.sharding import PartitionSpec as P

MESH = pl.DeviceIdType.MESH
epsilon = 1e-06
halo_depth = 16
block_rows = 16


def dot32(a, b):
    return jnp.dot(a, b, preferred_element_type=jnp.float32)


def iota(shape, dim):
    return lax.broadcasted_iota(jnp.int32, shape, dim)


def ones_where(mask):
    return jnp.where(mask, 1.0, 0.0).astype(jnp.bfloat16)


def kernel(
    n_ep,
    n_tp,
    cap,
    x_hbm,
    gain_ref,
    routes_ref,
    routes_t_ref,
    weight_ref,
    gate_hbm,
    up_hbm,
    down_hbm,
    pool_hbm,
    map_hbm,
    scale_ref,
    proj_hbm,
    pool_out,
    expert_out,
    x_v,
    gate_v,
    up_v,
    down_v,
    pool_v,
    map_v,
    proj_v,
    halo_v,
    stacked,
    xs,
    xd,
    yd,
    ys,
    yr,
    xr,
    rows_v,
    perm,
    perm_t,
    total,
    ext,
    sums,
    gathered,
    local_sem,
    halo_sem,
    xs_sem,
    xd_sem,
    yf_sem,
    yd_sem,
    ys_sem,
    yr_sem,
    xb_sem,
    xr_sem,
    ring_send,
    ring_recv,
):
    ep = lax.axis_index("ep")
    tp = lax.axis_index("tp")
    half = n_tp // 2
    rows, width = x_v.shape
    quarters = block_rows // cap
    lanes = width // quarters
    span = n_ep * block_rows
    part = n_ep * cap

    def offset(b, h):
        return (b + 1) % half if h == 0 else n_tp - (b + 1)

    def twin(b, h):
        return 2 * b + (1 - h) if b < half - 1 else 2 * b + h

    barrier = pltpu.get_barrier_semaphore()
    for r in range(1, n_tp):
        pl.semaphore_signal(
            barrier, inc=1, device_id={"tp": lax.rem(tp + r, n_tp)}, device_id_type=MESH
        )

    def greet(r, carry):
        pl.semaphore_signal(
            barrier, inc=1, device_id={"ep": lax.rem(ep + r, n_ep)}, device_id_type=MESH
        )
        return carry

    lax.fori_loop(1, n_ep, greet, 0)

    loads = [
        pltpu.make_async_copy(x_hbm, x_v, local_sem.at[0]),
        pltpu.make_async_copy(pool_hbm, pool_v, local_sem.at[1]),
        pltpu.make_async_copy(map_hbm.at[tp], map_v, local_sem.at[2]),
        pltpu.make_async_copy(gate_hbm.at[0], gate_v, local_sem.at[3]),
        pltpu.make_async_copy(up_hbm.at[0], up_v, local_sem.at[4]),
        pltpu.make_async_copy(down_hbm.at[0], down_v, local_sem.at[5]),
        pltpu.make_async_copy(proj_hbm, proj_v, local_sem.at[6]),
    ]
    for load in loads:
        load.start()

    later = ones_where(iota((rows, rows), 0) < iota((rows, rows), 1))
    earlier = ones_where(iota((rows, rows), 0) > iota((rows, rows), 1))
    row_id, col_id = iota((span, span), 0), iota((span, span), 1)

    def home(v):
        return ((v // cap) % n_ep) * block_rows + (v // part) * cap + v % cap

    perm[...] = ones_where(home(row_id) == col_id)
    perm_t[...] = ones_where(row_id == home(col_id))

    loads[0].wait()
    widened = x_v[...].astype(jnp.float32)
    normed = (
        widened
        * lax.rsqrt(jnp.mean(widened * widened, axis=1, keepdims=True) + epsilon)
        * gain_ref[...]
    ).astype(jnp.bfloat16)
    for q in range(quarters):
        stacked[q * rows : (q + 1) * rows, :] = normed[:, q * lanes : (q + 1) * lanes]

    slot_row = iota((span, rows), 0)

    def build(slot, off):
        expert = (slot_row // block_rows) * n_tp + lax.rem(tp + off, n_tp)
        named = (routes_t_ref[0:1, :] == expert) | (routes_t_ref[1:2, :] == expert)
        before = dot32(ones_where(named), later)
        chosen = named & (before == (slot_row % cap).astype(jnp.float32))
        quarter = (slot_row // cap) % quarters
        selector = jnp.concatenate(
            [ones_where(chosen & (quarter == q)) for q in range(quarters)], axis=1
        )
        block = dot32(selector, stacked[...]).astype(jnp.bfloat16)
        xs[slot] = block.reshape(n_ep, block_rows, lanes)

    def send_x(b, h):
        pltpu.make_async_remote_copy(
            src_ref=xs.at[2 * b + h],
            dst_ref=xd.at[twin(b, h)],
            send_sem=xs_sem,
            recv_sem=xd_sem.at[twin(b, h)],
            device_id={"tp": lax.rem(tp + offset(b, h), n_tp)},
            device_id_type=MESH,
        ).start()

    def forward_y(slot, b, source):
        def one(r, carry):
            peer = lax.rem(ep + r, n_ep)
            pltpu.make_async_remote_copy(
                src_ref=source.at[slot, peer],
                dst_ref=yd.at[slot, ep],
                send_sem=yf_sem,
                recv_sem=yd_sem.at[b],
                device_id={"ep": peer},
                device_id_type=MESH,
            ).start()
            return carry

        lax.fori_loop(1, n_ep, one, 0)
        yd[slot, ep] = source[slot, ep]

    def wait_bytes(ref, sem):
        pltpu.make_async_copy(ref, ref, sem).wait()

    own = 2 * (half - 1)
    order = [(b, h) for b in range(half) for h in range(2) if 2 * b + h != own]
    build(2 * order[0][0] + order[0][1], offset(*order[0]))
    pl.semaphore_wait(barrier, n_tp - 1 + n_ep - 1)
    halo = pltpu.make_async_remote_copy(
        src_ref=pool_v.at[pool_v.shape[0] - halo_depth :],
        dst_ref=halo_v,
        send_sem=halo_sem.at[0],
        recv_sem=halo_sem.at[1],
        device_id={"ep": lax.rem(ep + 1, n_ep)},
        device_id_type=MESH,
    )
    build(2 * order[1][0] + order[1][1], offset(*order[1]))
    send_x(*order[0])
    build(own, 0)
    send_x(*order[1])
    loads[1].wait()
    halo.start()
    for n, (b, h) in enumerate(order[2:]):
        build(2 * b + h, offset(b, h))
        if n == 0:
            forward_y(own, half - 1, xs)
        else:
            send_x(*order[n + 1])
    send_x(*order[-1])

    loads[2].wait()
    positions, channels = pool_v.shape
    ext[halo_depth:, :] = pool_v[...].astype(jnp.float32)
    halo.wait_recv()
    halo_rows = halo_v[...].astype(jnp.float32)
    ext[0:halo_depth, :] = jnp.where(ep == 0, jnp.zeros_like(halo_rows), halo_rows)
    level = lax.rem(tp, 4)
    summed = ext[halo_depth:, :] + ext[halo_depth - 1 : -1, :]
    sums[0, halo_depth:, :] = summed
    sums[0, 1:halo_depth, :] = ext[1:halo_depth, :] + ext[0 : halo_depth - 1, :]
    reach = 2
    first = 1
    for n in range(3):
        first = first + reach
        wider = sums[n, first:, :] + sums[n, first - reach : -reach, :]
        if n < 2:
            sums[n + 1, first:, :] = wider
        summed = jnp.where(level > n, wider[halo_depth - first :], summed)
        reach = 2 * reach
    window = jnp.left_shift(2, level)
    position = ep * positions + iota((positions, channels), 0)
    counted = jnp.minimum(position + 1, window).astype(jnp.float32)
    pooled = (summed / counted - ext[halo_depth:, :]).astype(jnp.bfloat16)
    mapped = dot32(pooled, map_v[...]) * scale_ref[tp]
    gathered[tp] = mapped.astype(jnp.bfloat16)

    def ring(step, way):
        block = lax.rem(tp + n_tp - way * (step - 1), n_tp)
        lane = (1 - way) // 2
        return pltpu.make_async_remote_copy(
            src_ref=gathered.at[block],
            dst_ref=gathered.at[block],
            send_sem=ring_send.at[lane, step - 1],
            recv_sem=ring_recv.at[lane, step - 1],
            device_id={"tp": lax.rem(tp + n_tp + way, n_tp)},
            device_id_type=MESH,
        )

    def relay(b):
        for h in range(2):
            wait_bytes(xd.at[2 * b + h], xd_sem.at[2 * b + h])
            forward_y(2 * b + h, b, xd)

    relay(0)
    for load in loads[3:6]:
        load.wait()
    ring(1, 1).start()
    ring(1, -1).start()

    def send_back(b, last):
        for h in range(2):
            slot = 2 * b + h
            if last and slot == own:
                continue
            target = slot if last else 2 * b + (1 - h)
            off = half * h if last else (b + 1 if h == 0 else n_tp - 1 - b)
            pltpu.make_async_remote_copy(
                src_ref=yr.at[slot],
                dst_ref=xr.at[target],
                send_sem=xb_sem,
                recv_sem=xr_sem.at[target],
                device_id={"tp": lax.rem(tp + off, n_tp)},
                device_id_type=MESH,
            ).start()

    def experts(b, carry):
        @pl.when(b < half - 2)
        def _():
            for h in range(2):
                slot = 2 * (b + 1) + h
                wait_bytes(xd.at[slot], xd_sem.at[slot])
                forward_y(slot, b + 1, xd)

        @pl.when(b == half - 2)
        def _():
            wait_bytes(xd.at[own + 1], xd_sem.at[own + 1])
            forward_y(own + 1, half - 1, xd)

        wait_bytes(yd.at[pl.ds(2 * b, 2), pl.ds(0, n_ep - 1)], yd_sem.at[b])
        for h in range(2):
            block = yd[2 * b + h].reshape(span, lanes)
            ordered = dot32(perm[...], block).astype(jnp.bfloat16)
            for q in range(quarters):
                rows_v[h * part : (h + 1) * part, q * lanes : (q + 1) * lanes] = ordered[
                    q * part : (q + 1) * part, :
                ]
        gate = dot32(rows_v[...], gate_v[...])
        up = dot32(rows_v[...], up_v[...])
        hidden = (gate / (1.0 + jnp.exp(-gate)) * up).astype(jnp.bfloat16)
        result = dot32(hidden, down_v[...]).astype(jnp.bfloat16)
        for h in range(2):
            tall = jnp.concatenate(
                [
                    result[h * part : (h + 1) * part, q * lanes : (q + 1) * lanes]
                    for q in range(quarters)
                ],
                axis=0,
            )
            block = dot32(perm_t[...], tall).astype(jnp.bfloat16)
            ys[2 * b + h] = block.reshape(n_ep, block_rows, lanes)
        for h in range(2):
            yr[2 * b + h, ep] = ys[2 * b + h, ep]

        def one(r, c):
            peer = lax.rem(ep + r, n_ep)
            pltpu.make_async_remote_copy(
                src_ref=ys.at[pl.ds(2 * b, 2), peer],
                dst_ref=yr.at[pl.ds(2 * b, 2), ep],
                send_sem=ys_sem,
                recv_sem=yr_sem.at[b],
                device_id={"ep": peer},
                device_id_type=MESH,
            ).start()
            return c

        lax.fori_loop(1, n_ep, one, 0)

        @pl.when(b >= 1)
        def _():
            wait_bytes(yr.at[pl.ds(2 * (b - 1), 2), pl.ds(0, n_ep - 1)], yr_sem.at[b - 1])
            send_back(b - 1, False)

        ring(b + 1, 1).wait_recv()

        @pl.when(b < half - 1)
        def _():
            ring(b + 2, 1).start()
            ring(b + 1, -1).wait_recv()

        @pl.when(b < half - 2)
        def _():
            ring(b + 2, -1).start()

        return carry

    lax.fori_loop(0, half, experts, 0)
    wait_bytes(
        yr.at[pl.ds(own, 2), pl.ds(0, n_ep - 1)], yr_sem.at[half - 1]
    )
    send_back(half - 1, True)

    loads[6].wait()
    tile = positions // 4

    def project(n, carry):
        at = pl.ds(pl.multiple_of(n * tile, tile), tile)
        left = jnp.concatenate([gathered[j, at, :] for j in range(n_tp)], axis=1)
        pool_out[at, :] = dot32(left, proj_v[...]).astype(jnp.bfloat16)
        return carry

    lax.fori_loop(0, 4, project, 0)

    total[...] = jnp.zeros_like(total)
    lane_id = iota((rows, span), 1)

    def combine(off, source, slot):
        expert = (lane_id // block_rows) * n_tp + lax.rem(tp + off, n_tp)
        named_0 = routes_ref[:, 0:1] == expert
        named_1 = routes_ref[:, 1:2] == expert
        before = dot32(earlier, ones_where(named_0 | named_1))
        hit = before == (lane_id % cap).astype(jnp.float32)
        quarter = (lane_id // cap) % quarters
        block = source[slot].reshape(span, lanes)
        for q in range(quarters):
            here = hit & (quarter == q)
            picker = jnp.concatenate(
                [ones_where(named_0 & here), ones_where(named_1 & here)], axis=0
            )
            picked = dot32(picker, block)
            total[:, q * lanes : (q + 1) * lanes] += (
                picked[:rows] * weight_ref[:, 0:1] + picked[rows:] * weight_ref[:, 1:2]
            )

    combine(0, yr, own)

    def collect(slot, carry):
        b, h = slot // 2, slot % 2
        off = jnp.where(h == 0, b + 1, n_tp - 1 - b)
        wait_bytes(xr.at[slot], xr_sem.at[slot])
        combine(off, xr, slot)
        return carry

    lax.fori_loop(0, own, collect, 0)
    wait_bytes(xr.at[own + 1], xr_sem.at[own + 1])
    combine(half, xr, own + 1)
    expert_out[...] = total[...].astype(jnp.bfloat16)

    halo.wait_send()
    wait_bytes(xs.at[pl.ds(0, n_tp - 1)], xs_sem)
    wait_bytes(yd.at[:, pl.ds(0, n_ep - 1)], yf_sem)
    wait_bytes(ys.at[:, pl.ds(0, n_ep - 1)], ys_sem)
    wait_bytes(yr.at[pl.ds(0, n_tp - 1)], xb_sem)
    for step in range(1, half + 1):
        ring(step, 1).wait_send()
        if step < half:
            ring(step, -1).wait_send()


def on_device(
    pool_input,
    pool_map,
    pool_scale,
    out_weight,
    expert_input,
    norm_gain,
    routes,
    route_weight,
    gate_weight,
    up_weight,
    down_weight,
):
    n_ep, n_tp = lax.axis_size("ep"), lax.axis_size("tp")
    rows, width = expert_input.shape
    positions, channels = pool_input.shape
    hidden = gate_weight.shape[2]
    features = out_weight.shape[1]
    cap = 2 * rows * routes.shape[1] // (n_ep * n_tp)
    quarters = block_rows // cap
    lanes = width // quarters
    span = n_ep * block_rows
    half = n_tp // 2
    routes_t = jnp.pad(routes.T, ((0, 8 - routes.shape[1]), (0, 0)), constant_values=-1)
    vmem = pl.BlockSpec(memory_space=pltpu.VMEM)
    anywhere = pl.BlockSpec(memory_space=pl.ANY)
    bf16, f32 = jnp.bfloat16, jnp.float32
    exchange = pltpu.VMEM((n_tp, n_ep, block_rows, lanes), bf16)
    dma = pltpu.SemaphoreType.DMA
    return pl.pallas_call(
        functools.partial(kernel, n_ep, n_tp, cap),
        out_shape=(
            jax.ShapeDtypeStruct((positions, features), bf16),
            jax.ShapeDtypeStruct((rows, width), bf16),
        ),
        in_specs=[
            anywhere,
            vmem,
            vmem,
            vmem,
            vmem,
            anywhere,
            anywhere,
            anywhere,
            anywhere,
            anywhere,
            vmem,
            anywhere,
        ],
        out_specs=(vmem, vmem),
        scratch_shapes=[
            pltpu.VMEM((rows, width), bf16),
            pltpu.VMEM((width, hidden), bf16),
            pltpu.VMEM((width, hidden), bf16),
            pltpu.VMEM((hidden, width), bf16),
            pltpu.VMEM((positions, channels), bf16),
            pltpu.VMEM((channels, channels), bf16),
            pltpu.VMEM(out_weight.shape, bf16),
            pltpu.VMEM((halo_depth, channels), bf16),
            pltpu.VMEM((quarters * rows, lanes), bf16),
            exchange,
            exchange,
            exchange,
            exchange,
            exchange,
            exchange,
            pltpu.VMEM((2 * n_ep * cap, width), bf16),
            pltpu.VMEM((span, span), bf16),
            pltpu.VMEM((span, span), bf16),
            pltpu.VMEM((rows, width), f32),
            pltpu.VMEM((positions + halo_depth, channels), f32),
            pltpu.VMEM((3, positions + halo_depth, channels), f32),
            pltpu.VMEM((n_tp, positions, channels), bf16),
            dma((7,)),
            dma((2,)),
            dma,
            dma((n_tp,)),
            dma,
            dma((half,)),
            dma,
            dma((half,)),
            dma,
            dma((n_tp,)),
            dma((2, half)),
            dma((2, half)),
        ],
        compiler_params=pltpu.CompilerParams(
            collective_id=0, has_side_effects=True, vmem_limit_bytes=56 * 1024 * 1024
        ),
    )(
        expert_input,
        norm_gain.reshape(1, width),
        routes,
        routes_t,
        route_weight,
        gate_weight,
        up_weight,
        down_weight,
        pool_input,
        pool_map,
        pool_scale.reshape(n_tp, 1, channels),
        out_weight,
    )


def solution(mesh):
    return jax.shard_map(
        on_device,
        mesh=mesh,
        in_specs=(
            P(("grp", "ep"), "tp"),
            P(),
            P(),
            P(None, "tp"),
            P(("grp", "ep", "tp"), None),
            P(),
            P(("grp", "ep", "tp"), None),
            P(("grp", "ep", "tp"), None),
            P(("ep", "tp"), None, None),
            P(("ep", "tp"), None, None),
            P(("ep", "tp"), None, None),
        ),
        out_specs=(P(("grp", "ep"), "tp"), P(("grp", "ep", "tp"), None)),
        check_vma=False,
    )
```

time: 224 us -> 166 us (0.74)
  the two profiles are of different devices: /device:TPU:528 before, /device:TPU:517 now
where the time goes in v1:
time: 166 us; the launch traced here: 165 us
  Pallas kernels  157 us (95%)
  local copies, waits for them, and re-layouts  7.85 us (5%)
    pallas_call x1, Pallas kernels, on_device(): pl.pallas_call(functools.partial(kernel, n_ep, n_tp, cap), out_shape=(jax...  157 us
    unnamed x4, local copies, waits for them, and re-layouts  6.57 us

profile of v1, /device:TPU:517, one launch (start us, length us, event | category | flops | bytes accessed | tf_op | source)
XLA Modules:
  0.0 165.2 jit_solution(66081221670476799)
XLA Ops:
  0.6 1.3 pad.4.routes_t_ref
  1.9 1.4 copy.14.weight_ref
  3.3 1.4 copy.13.routes_ref
  4.7 156.8 %shard_map.122 = (bf16[1024,256]{1,0:T(8,128)(2,1)}, bf16[128,2048]{1,0:T(8,128)(2,1)}) custom-call(bf16[128,2048]{1,0:T(8,128)(2,1)} %x_hbm.1, f32[1,2048]{1,0:T(1,128)} %bitcast.3, s32[128,2]{1,0:T(8,128)} %copy.13.routes_ref, s32[8,128]{1,0:T(8,128)} %pad.4.routes_t_ref, f32[128,2]{1,0:T(8,128)} %copy.14.weight_ref, bf16[1,2048,512]{2,1,0:T(8,128)(2,1)} %gate_hbm.1, ...), custom_call_target="tpu_custom_call" | custom-call | tf_op jit(solution)/shard_map/pallas_call | solution.py:438
  161.5 1.9 %copy.17 = bf16[1024,256]{1,0:T(8,128)(2,1)} copy(bf16[1024,256]{1,0:T(8,128)(2,1)} %get-tuple-element.4) | data formatting | bytes 1048576
  163.4 1.9 %copy.18 = bf16[128,2048]{1,0:T(8,128)(2,1)} copy(bf16[128,2048]{1,0:T(8,128)(2,1)} %get-tuple-element.5) | data formatting | bytes 1048576

commit v2 on v1

--- a/solution.py
+++ b/solution.py
@@ -11,6 +11,8 @@
 epsilon = 1e-06
 halo_depth = 16
 block_rows = 16
+pairs = ((2, 6), (1, 7), (3, 5), (4, 0))
+agenda = ("r0", "r1", "e0", "r2", "s1", "k0", "r3", "w1", "s2", "e2", "w2", "s3", "e3", "w3", "s4", "e1", "k2", "k3", "k1", "w4")
 
 
 def dot32(a, b):
@@ -30,19 +32,22 @@
     n_tp,
     cap,
     x_hbm,
-    gain_ref,
-    routes_ref,
-    routes_t_ref,
-    weight_ref,
+    gain_hbm,
+    routes_hbm,
+    weight_hbm,
     gate_hbm,
     up_hbm,
     down_hbm,
     pool_hbm,
     map_hbm,
-    scale_ref,
+    scale_hbm,
     proj_hbm,
     pool_out,
     expert_out,
+    gain_ref,
+    routes_ref,
+    weight_ref,
+    scale_ref,
     x_v,
     gate_v,
     up_v,
@@ -87,11 +92,13 @@
     span = n_ep * block_rows
     part = n_ep * cap
 
-    def offset(b, h):
-        return (b + 1) % half if h == 0 else n_tp - (b + 1)
-
-    def twin(b, h):
-        return 2 * b + (1 - h) if b < half - 1 else 2 * b + h
+    own = [off for pair in pairs for off in pair].index(0)
+
+    def offset(slot):
+        return pairs[slot // 2][slot % 2]
+
+    def twin(slot):
+        return slot if slot // 2 == own // 2 else slot ^ 1
 
     barrier = pltpu.get_barrier_semaphore()
     for r in range(1, n_tp):
@@ -107,14 +114,22 @@
 
     lax.fori_loop(1, n_ep, greet, 0)
 
+    moves = [
+        (x_hbm, x_v),
+        (gain_hbm, gain_ref),
+        (routes_hbm, routes_ref),
+        (pool_hbm, pool_v),
+        (map_hbm.at[tp], map_v),
+        (scale_hbm.at[tp], scale_ref),
+        (gate_hbm.at[0], gate_v),
+        (up_hbm.at[0], up_v),
+        (down_hbm.at[0], down_v),
+        (proj_hbm, proj_v),
+        (weight_hbm, weight_ref),
+    ]
     loads = [
-        pltpu.make_async_copy(x_hbm, x_v, local_sem.at[0]),
-        pltpu.make_async_copy(pool_hbm, pool_v, local_sem.at[1]),
-        pltpu.make_async_copy(map_hbm.at[tp], map_v, local_sem.at[2]),
-        pltpu.make_async_copy(gate_hbm.at[0], gate_v, local_sem.at[3]),
-        pltpu.make_async_copy(up_hbm.at[0], up_v, local_sem.at[4]),
-        pltpu.make_async_copy(down_hbm.at[0], down_v, local_sem.at[5]),
-        pltpu.make_async_copy(proj_hbm, proj_v, local_sem.at[6]),
+        pltpu.make_async_copy(source, target, local_sem.at[n])
+        for n, (source, target) in enumerate(moves)
     ]
     for load in loads:
         load.start()
@@ -129,7 +144,8 @@
     perm[...] = ones_where(home(row_id) == col_id)
     perm_t[...] = ones_where(row_id == home(col_id))
 
-    loads[0].wait()
+    for load in loads[:3]:
+        load.wait()
     widened = x_v[...].astype(jnp.float32)
     normed = (
         widened
@@ -143,7 +159,7 @@
 
     def build(slot, off):
         expert = (slot_row // block_rows) * n_tp + lax.rem(tp + off, n_tp)
-        named = (routes_t_ref[0:1, :] == expert) | (routes_t_ref[1:2, :] == expert)
+        named = (routes_ref[0:1, :] == expert) | (routes_ref[1:2, :] == expert)
         before = dot32(ones_where(named), later)
         chosen = named & (before == (slot_row % cap).astype(jnp.float32))
         quarter = (slot_row // cap) % quarters
@@ -153,24 +169,24 @@
         block = dot32(selector, stacked[...]).astype(jnp.bfloat16)
         xs[slot] = block.reshape(n_ep, block_rows, lanes)
 
-    def send_x(b, h):
+    def send_x(slot):
         pltpu.make_async_remote_copy(
-            src_ref=xs.at[2 * b + h],
-            dst_ref=xd.at[twin(b, h)],
+            src_ref=xs.at[slot],
+            dst_ref=xd.at[twin(slot)],
             send_sem=xs_sem,
-            recv_sem=xd_sem.at[twin(b, h)],
-            device_id={"tp": lax.rem(tp + offset(b, h), n_tp)},
+            recv_sem=xd_sem.at[twin(slot)],
+            device_id={"tp": lax.rem(tp + offset(slot), n_tp)},
             device_id_type=MESH,
         ).start()
 
-    def forward_y(slot, b, source):
+    def forward_y(slot, source):
         def one(r, carry):
             peer = lax.rem(ep + r, n_ep)
             pltpu.make_async_remote_copy(
                 src_ref=source.at[slot, peer],
                 dst_ref=yd.at[slot, ep],
                 send_sem=yf_sem,
-                recv_sem=yd_sem.at[b],
+                recv_sem=yd_sem.at[slot // 2],
                 device_id={"ep": peer},
                 device_id_type=MESH,
             ).start()
@@ -179,13 +195,14 @@
         lax.fori_loop(1, n_ep, one, 0)
         yd[slot, ep] = source[slot, ep]
 
-    def wait_bytes(ref, sem):
-        pltpu.make_async_copy(ref, ref, sem).wait()
-
-    own = 2 * (half - 1)
-    order = [(b, h) for b in range(half) for h in range(2) if 2 * b + h != own]
-    build(2 * order[0][0] + order[0][1], offset(*order[0]))
-    pl.semaphore_wait(barrier, n_tp - 1 + n_ep - 1)
+    def wait_bytes(ref, sem, name="drain"):
+        with jax.named_scope(name):
+            pltpu.make_async_copy(ref, ref, sem).wait()
+
+    order = [slot for slot in range(n_tp) if slot != own]
+    build(order[0], offset(order[0]))
+    with jax.named_scope("barrier"):
+        pl.semaphore_wait(barrier, n_tp - 1 + n_ep - 1)
     halo = pltpu.make_async_remote_copy(
         src_ref=pool_v.at[pool_v.shape[0] - halo_depth :],
         dst_ref=halo_v,
@@ -194,24 +211,25 @@
         device_id={"ep": lax.rem(ep + 1, n_ep)},
         device_id_type=MESH,
     )
-    build(2 * order[1][0] + order[1][1], offset(*order[1]))
-    send_x(*order[0])
+    build(order[1], offset(order[1]))
+    send_x(order[0])
     build(own, 0)
-    send_x(*order[1])
-    loads[1].wait()
+    send_x(order[1])
+    loads[3].wait()
     halo.start()
-    for n, (b, h) in enumerate(order[2:]):
-        build(2 * b + h, offset(b, h))
-        if n == 0:
-            forward_y(own, half - 1, xs)
-        else:
-            send_x(*order[n + 1])
-    send_x(*order[-1])
-
-    loads[2].wait()
+    build(order[2], offset(order[2]))
+    forward_y(own, xs)
+    for n in range(3, len(order)):
+        build(order[n], offset(order[n]))
+        send_x(order[n - 1])
+    send_x(order[-1])
+
+    for load in loads[4:6]:
+        load.wait()
     positions, channels = pool_v.shape
     ext[halo_depth:, :] = pool_v[...].astype(jnp.float32)
-    halo.wait_recv()
+    with jax.named_scope("halo"):
+        halo.wait_recv()
     halo_rows = halo_v[...].astype(jnp.float32)
     ext[0:halo_depth, :] = jnp.where(ep == 0, jnp.zeros_like(halo_rows), halo_rows)
     level = lax.rem(tp, 4)
@@ -231,7 +249,7 @@
     position = ep * positions + iota((positions, channels), 0)
     counted = jnp.minimum(position + 1, window).astype(jnp.float32)
     pooled = (summed / counted - ext[halo_depth:, :]).astype(jnp.bfloat16)
-    mapped = dot32(pooled, map_v[...]) * scale_ref[tp]
+    mapped = dot32(pooled, map_v[...]) * scale_ref[...]
     gathered[tp] = mapped.astype(jnp.bfloat16)
 
     def ring(step, way):
@@ -247,46 +265,26 @@
         )
 
     def relay(b):
-        for h in range(2):
-            wait_bytes(xd.at[2 * b + h], xd_sem.at[2 * b + h])
-            forward_y(2 * b + h, b, xd)
-
-    relay(0)
-    for load in loads[3:6]:
-        load.wait()
-    ring(1, 1).start()
-    ring(1, -1).start()
-
-    def send_back(b, last):
-        for h in range(2):
-            slot = 2 * b + h
-            if last and slot == own:
-                continue
-            target = slot if last else 2 * b + (1 - h)
-            off = half * h if last else (b + 1 if h == 0 else n_tp - 1 - b)
-            pltpu.make_async_remote_copy(
-                src_ref=yr.at[slot],
-                dst_ref=xr.at[target],
-                send_sem=xb_sem,
-                recv_sem=xr_sem.at[target],
-                device_id={"tp": lax.rem(tp + off, n_tp)},
-                device_id_type=MESH,
-            ).start()
-
-    def experts(b, carry):
-        @pl.when(b < half - 2)
-        def _():
-            for h in range(2):
-                slot = 2 * (b + 1) + h
-                wait_bytes(xd.at[slot], xd_sem.at[slot])
-                forward_y(slot, b + 1, xd)
-
-        @pl.when(b == half - 2)
-        def _():
-            wait_bytes(xd.at[own + 1], xd_sem.at[own + 1])
-            forward_y(own + 1, half - 1, xd)
-
-        wait_bytes(yd.at[pl.ds(2 * b, 2), pl.ds(0, n_ep - 1)], yd_sem.at[b])
+        for slot in (2 * b, 2 * b + 1):
+            if slot != own:
+                wait_bytes(xd.at[slot], xd_sem.at[slot], f"xd_{slot}")
+                forward_y(slot, xd)
+
+    def send_back(b):
+        for slot in (2 * b, 2 * b + 1):
+            wait_bytes(yr.at[slot, pl.ds(0, n_ep - 1)], yr_sem.at[slot], f"yr_{slot}")
+            if slot != own:
+                pltpu.make_async_remote_copy(
+                    src_ref=yr.at[slot],
+                    dst_ref=xr.at[twin(slot)],
+                    send_sem=xb_sem,
+                    recv_sem=xr_sem.at[twin(slot)],
+                    device_id={"tp": lax.rem(tp + offset(slot), n_tp)},
+                    device_id_type=MESH,
+                ).start()
+
+    def experts(b):
+        wait_bytes(yd.at[pl.ds(2 * b, 2), pl.ds(0, n_ep - 1)], yd_sem.at[b], f"yd_{b}")
         for h in range(2):
             block = yd[2 * b + h].reshape(span, lanes)
             ordered = dot32(perm[...], block).astype(jnp.bfloat16)
@@ -311,45 +309,44 @@
         for h in range(2):
             yr[2 * b + h, ep] = ys[2 * b + h, ep]
 
-        def one(r, c):
-            peer = lax.rem(ep + r, n_ep)
+        def one(n, c):
+            h = n // (n_ep - 1)
+            peer = lax.rem(ep + 1 + n - h * (n_ep - 1), n_ep)
             pltpu.make_async_remote_copy(
-                src_ref=ys.at[pl.ds(2 * b, 2), peer],
-                dst_ref=yr.at[pl.ds(2 * b, 2), ep],
+                src_ref=ys.at[2 * b + h, peer],
+                dst_ref=yr.at[2 * b + h, ep],
                 send_sem=ys_sem,
-                recv_sem=yr_sem.at[b],
+                recv_sem=yr_sem.at[2 * b + h],
                 device_id={"ep": peer},
                 device_id_type=MESH,
             ).start()
             return c
 
-        lax.fori_loop(1, n_ep, one, 0)
-
-        @pl.when(b >= 1)
-        def _():
-            wait_bytes(yr.at[pl.ds(2 * (b - 1), 2), pl.ds(0, n_ep - 1)], yr_sem.at[b - 1])
-            send_back(b - 1, False)
-
-        ring(b + 1, 1).wait_recv()
-
-        @pl.when(b < half - 1)
-        def _():
-            ring(b + 2, 1).start()
-            ring(b + 1, -1).wait_recv()
-
-        @pl.when(b < half - 2)
-        def _():
-            ring(b + 2, -1).start()
-
-        return carry
-
-    lax.fori_loop(0, half, experts, 0)
-    wait_bytes(
-        yr.at[pl.ds(own, 2), pl.ds(0, n_ep - 1)], yr_sem.at[half - 1]
-    )
-    send_back(half - 1, True)
-
-    loads[6].wait()
+        lax.fori_loop(0, 2 * (n_ep - 1), one, 0)
+
+    def ring_start(step):
+        ring(step, 1).start()
+        if step < half:
+            ring(step, -1).start()
+
+    def ring_wait(step):
+        with jax.named_scope(f"ring_{step}"):
+            ring(step, 1).wait_recv()
+            if step < half:
+                ring(step, -1).wait_recv()
+
+    for load in loads[6:]:
+        load.wait()
+    calls = {
+        "r": relay,
+        "e": experts,
+        "k": send_back,
+        "s": ring_start,
+        "w": ring_wait,
+    }
+    for step in agenda:
+        calls[step[0]](int(step[1]))
+
     tile = positions // 4
 
     def project(n, carry):
@@ -363,10 +360,16 @@
     total[...] = jnp.zeros_like(total)
     lane_id = iota((rows, span), 1)
 
+    def upright(ref, k):
+        return jnp.broadcast_to(ref[k : k + 1, :], (rows, rows)).T[:, 0:1]
+
+    expert_0, expert_1 = upright(routes_ref, 0), upright(routes_ref, 1)
+    weight_0, weight_1 = upright(weight_ref, 0), upright(weight_ref, 1)
+
     def combine(off, source, slot):
         expert = (lane_id // block_rows) * n_tp + lax.rem(tp + off, n_tp)
-        named_0 = routes_ref[:, 0:1] == expert
-        named_1 = routes_ref[:, 1:2] == expert
+        named_0 = expert_0 == expert
+        named_1 = expert_1 == expert
         before = dot32(earlier, ones_where(named_0 | named_1))
         hit = before == (lane_id % cap).astype(jnp.float32)
         quarter = (lane_id // cap) % quarters
@@ -378,21 +381,13 @@
             )
             picked = dot32(picker, block)
             total[:, q * lanes : (q + 1) * lanes] += (
-                picked[:rows] * weight_ref[:, 0:1] + picked[rows:] * weight_ref[:, 1:2]
+                picked[:rows] * weight_0 + picked[rows:] * weight_1
             )
 
     combine(0, yr, own)
-
-    def collect(slot, carry):
-        b, h = slot // 2, slot % 2
-        off = jnp.where(h == 0, b + 1, n_tp - 1 - b)
-        wait_bytes(xr.at[slot], xr_sem.at[slot])
-        combine(off, xr, slot)
-        return carry
-
-    lax.fori_loop(0, own, collect, 0)
-    wait_bytes(xr.at[own + 1], xr_sem.at[own + 1])
-    combine(half, xr, own + 1)
+    for slot in order:
+        wait_bytes(xr.at[slot], xr_sem.at[slot], f"xr_{slot}")
+        combine(offset(slot), xr, slot)
     expert_out[...] = total[...].astype(jnp.bfloat16)
 
     halo.wait_send()
@@ -404,6 +399,10 @@
         ring(step, 1).wait_send()
         if step < half:
             ring(step, -1).wait_send()
+
+
+def held(array):
+    return pltpu.with_memory_space_constraint(array, pltpu.HBM)
 
 
 def on_device(
@@ -429,9 +428,8 @@
     lanes = width // quarters
     span = n_ep * block_rows
     half = n_tp // 2
-    routes_t = jnp.pad(routes.T, ((0, 8 - routes.shape[1]), (0, 0)), constant_values=-1)
     vmem = pl.BlockSpec(memory_space=pltpu.VMEM)
-    anywhere = pl.BlockSpec(memory_space=pl.ANY)
+    far = pl.BlockSpec(memory_space=pl.ANY)
     bf16, f32 = jnp.bfloat16, jnp.float32
     exchange = pltpu.VMEM((n_tp, n_ep, block_rows, lanes), bf16)
     dma = pltpu.SemaphoreType.DMA
@@ -441,22 +439,13 @@
             jax.ShapeDtypeStruct((positions, features), bf16),
             jax.ShapeDtypeStruct((rows, width), bf16),
         ),
-        in_specs=[
-            anywhere,
-            vmem,
-            vmem,
-            vmem,
-            vmem,
-            anywhere,
-            anywhere,
-            anywhere,
-            anywhere,
-            anywhere,
-            vmem,
-            anywhere,
-        ],
+        in_specs=[far] * 11,
         out_specs=(vmem, vmem),
         scratch_shapes=[
+            pltpu.VMEM((1, width), f32),
+            pltpu.VMEM(routes.T.shape, jnp.int32),
+            pltpu.VMEM(routes.T.shape, f32),
+            pltpu.VMEM((1, channels), f32),
             pltpu.VMEM((rows, width), bf16),
             pltpu.VMEM((width, hidden), bf16),
             pltpu.VMEM((width, hidden), bf16),
@@ -479,35 +468,39 @@
             pltpu.VMEM((positions + halo_depth, channels), f32),
             pltpu.VMEM((3, positions + halo_depth, channels), f32),
             pltpu.VMEM((n_tp, positions, channels), bf16),
-            dma((7,)),
+            dma((11,)),
             dma((2,)),
             dma,
             dma((n_tp,)),
             dma,
             dma((half,)),
             dma,
-            dma((half,)),
+            dma((n_tp,)),
             dma,
             dma((n_tp,)),
             dma((2, half)),
             dma((2, half)),
         ],
         compiler_params=pltpu.CompilerParams(
-            collective_id=0, has_side_effects=True, vmem_limit_bytes=56 * 1024 * 1024
+            collective_id=0, has_side_effects=True, vmem_limit_bytes=50 * 1024 * 1024
         ),
     )(
-        expert_input,
-        norm_gain.reshape(1, width),
-        routes,
-        routes_t,
-        route_weight,
-        gate_weight,
-        up_weight,
-        down_weight,
-        pool_input,
-        pool_map,
-        pool_scale.reshape(n_tp, 1, channels),
-        out_weight,
+        *map(
+            held,
+            (
+                expert_input,
+                norm_gain.reshape(1, width),
+                routes.T,
+                route_weight.T,
+                gate_weight,
+                up_weight,
+                down_weight,
+                pool_input,
+                pool_map,
+                pool_scale.reshape(n_tp, 1, channels),
+                out_weight,
+            ),
+        )
     )
 
 

time: 166 us -> 145 us (0.87)
  the two profiles are of different devices: /device:TPU:517 before, /device:TPU:528 now
where the time goes in v2:
time: 145 us
  Pallas kernels  142 us (98%)
  local copies, waits for them, and re-layouts  1.59 us (1%)
    pallas_call x1, Pallas kernels, on_device(): pl.pallas_call(functools.partial(kernel, n_ep, n_tp, cap), out_shape=(jax...  142 us

profile of v2, /device:TPU:528, one launch (start us, length us, event | category | flops | bytes accessed | tf_op | source)
XLA Modules:
  0.0 144.5 jit_solution(10039917310650870010)
XLA Ops:
  0.6 142.3 %shard_map.122 = (bf16[1024,256]{1,0:T(8,128)(2,1)S(1)}, bf16[128,2048]{1,0:T(8,128)(2,1)S(1)}) custom-call(bf16[128,2048]{1,0:T(8,128)(2,1)} %x_hbm.1, f32[1,2048]{1,0:T(1,128)} %bitcast.4, s32[2,128]{1,0:T(2,128)} %bitcast.6, f32[2,128]{1,0:T(2,128)} %bitcast.7, bf16[1,2048,512]{2,1,0:T(8,128)(2,1)} %gate_hbm.1, bf16[1,2048,512]{2,1,0:T(8,128)(2,1)} %up_hbm.1, ...), custom_call_target="tpu_custom_call" | custom-call | tf_op jit(solution)/shard_map/pallas_call | solution.py:436
  142.9 0.8 copy.15
  143.7 0.8 copy.16

commit v3 on v2

--- a/solution.py
+++ b/solution.py
@@ -12,7 +12,7 @@
 halo_depth = 16
 block_rows = 16
 pairs = ((2, 6), (1, 7), (3, 5), (4, 0))
-agenda = ("r0", "r1", "e0", "r2", "s1", "k0", "r3", "w1", "s2", "e2", "w2", "s3", "e3", "w3", "s4", "e1", "k2", "k3", "k1", "w4")
+agenda = ("r0", "r1", "e0", "r2", "s1", "k0", "r3", "w1", "s2", "e2", "w2", "s3", "e3", "k2", "w3", "s4", "e1", "k3", "k1", "w4")
 
 
 def dot32(a, b):
@@ -385,7 +385,10 @@
             )
 
     combine(0, yr, own)
-    for slot in order:
+    arrival = [2 * int(step[1]) + h for step in agenda if step[0] == "k" for h in range(2)]
+    for slot in arrival:
+        if slot == own:
+            continue
         wait_bytes(xr.at[slot], xr_sem.at[slot], f"xr_{slot}")
         combine(offset(slot), xr, slot)
     expert_out[...] = total[...].astype(jnp.bfloat16)

time: 145 us -> 140 us (0.966)
  Pallas kernels: 142 us -> 136 us
    pallas_call x1, Pallas kernels: 142 us -> 136 us  [on_device(): pl.pallas_call(functools.partial(kernel, n_ep, n_tp, cap), out_shape=(jax...]
where the time goes in v3:
time: 140 us; the launch traced here: 138 us
  Pallas kernels  136 us (97%)
  local copies, waits for them, and re-layouts  1.59 us (1%)
    pallas_call x1, Pallas kernels, on_device(): pl.pallas_call(functools.partial(kernel, n_ep, n_tp, cap), out_shape=(jax...  136 us

profile of v3, /device:TPU:528, one launch (start us, length us, event | category | flops | bytes accessed | tf_op | source)
XLA Modules:
  0.0 138.2 jit_solution(14112770012681039139)
XLA Ops:
  0.6 136.0 %shard_map.122 = (bf16[1024,256]{1,0:T(8,128)(2,1)S(1)}, bf16[128,2048]{1,0:T(8,128)(2,1)S(1)}) custom-call(bf16[128,2048]{1,0:T(8,128)(2,1)} %x_hbm.1, f32[1,2048]{1,0:T(1,128)} %bitcast.4, s32[2,128]{1,0:T(2,128)} %bitcast.6, f32[2,128]{1,0:T(2,128)} %bitcast.7, bf16[1,2048,512]{2,1,0:T(8,128)(2,1)} %gate_hbm.1, bf16[1,2048,512]{2,1,0:T(8,128)(2,1)} %up_hbm.1, ...), custom_call_target="tpu_custom_call" | custom-call | tf_op jit(solution)/shard_map/pallas_call | solution.py:439
  136.6 0.8 copy.15
  137.4 0.8 copy.16

commit v4 on v3

--- a/solution.py
+++ b/solution.py
@@ -12,7 +12,7 @@
 halo_depth = 16
 block_rows = 16
 pairs = ((2, 6), (1, 7), (3, 5), (4, 0))
-agenda = ("r0", "r1", "e0", "r2", "s1", "k0", "r3", "w1", "s2", "e2", "w2", "s3", "e3", "k2", "w3", "s4", "e1", "k3", "k1", "w4")
+agenda = ("r0", "r1", "e0", "s1", "r2", "w1", "s2", "k0", "r3", "e2", "w2", "s3", "e3", "k2", "w3", "s4", "e1", "k3", "k1", "w4")
 
 
 def dot32(a, b):

time: 140 us -> 138 us (0.986)
  Pallas kernels: 136 us -> 133 us
    pallas_call x1, Pallas kernels: 136 us -> 133 us  [on_device(): pl.pallas_call(functools.partial(kernel, n_ep, n_tp, cap), out_shape=(jax...]
where the time goes in v4:
time: 138 us; the launch traced here: 135 us
  Pallas kernels  133 us (96%)
  local copies, waits for them, and re-layouts  1.59 us (1%)
    pallas_call x1, Pallas kernels, on_device(): pl.pallas_call(functools.partial(kernel, n_ep, n_tp, cap), out_shape=(jax...  133 us

profile of v4, /device:TPU:528, one launch (start us, length us, event | category | flops | bytes accessed | tf_op | source)
XLA Modules:
  0.0 135.1 jit_solution(8058545519365391671)
XLA Ops:
  0.6 132.9 %shard_map.122 = (bf16[1024,256]{1,0:T(8,128)(2,1)S(1)}, bf16[128,2048]{1,0:T(8,128)(2,1)S(1)}) custom-call(bf16[128,2048]{1,0:T(8,128)(2,1)} %x_hbm.1, f32[1,2048]{1,0:T(1,128)} %bitcast.4, s32[2,128]{1,0:T(2,128)} %bitcast.6, f32[2,128]{1,0:T(2,128)} %bitcast.7, bf16[1,2048,512]{2,1,0:T(8,128)(2,1)} %gate_hbm.1, bf16[1,2048,512]{2,1,0:T(8,128)(2,1)} %up_hbm.1, ...), custom_call_target="tpu_custom_call" | custom-call | tf_op jit(solution)/shard_map/pallas_call | solution.py:439
  133.5 0.8 copy.15
  134.3 0.8 copy.16

commit v5 on v4

--- a/solution.py
+++ b/solution.py
@@ -12,7 +12,7 @@
 halo_depth = 16
 block_rows = 16
 pairs = ((2, 6), (1, 7), (3, 5), (4, 0))
-agenda = ("r0", "r1", "e0", "s1", "r2", "w1", "s2", "k0", "r3", "e2", "w2", "s3", "e3", "k2", "w3", "s4", "e1", "k3", "k1", "w4")
+agenda = ("r0", "r1", "e0", "s1", "r2", "w1", "s2", "k0", "r3", "e2", "w2", "s3", "e3", "k2", "w3", "s4", "e1", "k3", "k1")
 
 
 def dot32(a, b):
@@ -355,7 +355,6 @@
         pool_out[at, :] = dot32(left, proj_v[...]).astype(jnp.bfloat16)
         return carry
 
-    lax.fori_loop(0, 4, project, 0)
 
     total[...] = jnp.zeros_like(total)
     lane_id = iota((rows, span), 1)
@@ -389,6 +388,9 @@
     for slot in arrival:
         if slot == own:
             continue
+        if slot == arrival[-4]:
+            ring_wait(half)
+            lax.fori_loop(0, 4, project, 0)
         wait_bytes(xr.at[slot], xr_sem.at[slot], f"xr_{slot}")
         combine(offset(slot), xr, slot)
     expert_out[...] = total[...].astype(jnp.bfloat16)

time: 138 us -> 138 us (level)
  no operation moved by 1% of the time
where the time goes in v5:
time: 138 us; the launch traced here: 135 us
  Pallas kernels  133 us (96%)
  local copies, waits for them, and re-layouts  1.59 us (1%)
    pallas_call x1, Pallas kernels, on_device(): pl.pallas_call(functools.partial(kernel, n_ep, n_tp, cap), out_shape=(jax...  133 us

profile of v5, /device:TPU:528, one launch (start us, length us, event | category | flops | bytes accessed | tf_op | source)
XLA Modules:
  0.0 135.1 jit_solution(6144708264104120107)
XLA Ops:
  0.6 132.9 %shard_map.122 = (bf16[1024,256]{1,0:T(8,128)(2,1)S(1)}, bf16[128,2048]{1,0:T(8,128)(2,1)S(1)}) custom-call(bf16[128,2048]{1,0:T(8,128)(2,1)} %x_hbm.1, f32[1,2048]{1,0:T(1,128)} %bitcast.4, s32[2,128]{1,0:T(2,128)} %bitcast.6, f32[2,128]{1,0:T(2,128)} %bitcast.7, bf16[1,2048,512]{2,1,0:T(8,128)(2,1)} %gate_hbm.1, bf16[1,2048,512]{2,1,0:T(8,128)(2,1)} %up_hbm.1, ...), custom_call_target="tpu_custom_call" | custom-call | tf_op jit(solution)/shard_map/pallas_call | solution.py:441
  133.5 0.8 copy.15
  134.3 0.8 copy.16
